TPU v7x, 32 devices: a whole 2x2x4 slice. The times are simulated.
32 devices in a mesh: grp: 2 (over y), fs: 4 (over z), tp: 4 (over x, core).
Axes of the slice: x: 2, y: 2, z: 4, core: 2. Of those that a mesh axis runs over, the one named last changes fastest.
Arguments:
- tokens: bfloat16 [8192, 2048], P(('grp', 'fs'), 'tp'), parts along dimension 0, may hold values from -6 to 6
- norm1_gain: float32 [2048], replicated, may hold values from 0.1 to 1.9
- weight_u: float32 [2048, 1024], P('fs', 'tp'), may hold values from -0.125 to 0.125
- weight_v: float32 [2048, 1024], P('fs', 'tp'), may hold values from -0.125 to 0.125
- scale_u: float32 [1024], P('tp'), may hold values from 0.5 to 2
- scale_v: float32 [1024], P('tp'), may hold values from 0.05 to 4.5
- mix_gain: float32 [1024], P('tp'), may hold values from 0.1 to 1.9
- spatial_weight: float32 [4, 128, 128], replicated, may hold values from -0.5 to 0.5
- spatial_bias: float32 [4, 128], replicated, may hold values from 0.5 to 1.5
- weight_out: float32 [1024, 2048], P('tp', 'fs'), may hold values from -0.1875 to 0.1875
- scale_out: float32 [2048], P('fs'), may hold values from 0.5 to 2
- norm2_gain: float32 [2048], replicated, may hold values from 0.1 to 1.9
- weight_up: float32 [2048, 8192], P('fs', 'tp'), may hold values from -0.125 to 0.125
- scale_up: float32 [8192], P('tp'), may hold values from 0.5 to 2
- weight_down: float32 [8192, 2048], P('tp', 'fs'), may hold values from -0.0625 to 0.0625
- scale_down: float32 [2048], P('fs'), may hold values from 0.5 to 2
Outputs:
- result: bfloat16 [8192, 2048], P(('grp', 'fs'), 'tp'), parts along dimension 0
There are 2 independent parts, one for each index of `grp`. A program takes and returns all parts, laid end to end along the dimension named above; an argument that names none is the same for every part. Nothing has to cross between parts.
All inputs are finite; a program needn't handle non-finite values.
Results may differ from a plain program's by a relative error of at most 0.023.
Values may be sent and summed in bfloat16 or wider, within the bound.
A program may use at most 128 MiB of HBM per device.

v0:
```python
import jax
import jax.numpy as jnp
from jax import lax
from jax.sharding import PartitionSpec as P

GM_W = 1024
GROUPS = 4
BLOCK = 128


def per_device(
    tokens,
    norm1_gain,
    weight_u,
    weight_v,
    scale_u,
    scale_v,
    mix_gain,
    spatial_weight,
    spatial_bias,
    weight_out,
    scale_out,
    norm2_gain,
    weight_up,
    scale_up,
    weight_down,
    scale_down,
):
    feature_count = norm1_gain.shape[0]
    out_scales, down_scales = (
        lax.all_gather(scale_out, "fs", axis=0, tiled=True),
        lax.all_gather(scale_down, "fs", axis=0, tiled=True),
    )
    full_u, full_v = (
        lax.all_gather(weight_u.astype(jnp.bfloat16), "fs", axis=0, tiled=True),
        lax.all_gather(weight_v.astype(jnp.bfloat16), "fs", axis=0, tiled=True),
    )
    widened_in = tokens.astype(jnp.float32)
    squares_in = lax.psum(jnp.sum(widened_in * widened_in, axis=1), "tp")
    inverse_in = lax.rsqrt(squares_in / feature_count + 1e-06)[:, None]
    gain_piece = norm1_gain
    normed_piece = (
        lax.all_gather(tokens, "tp", axis=1, tiled=True).astype(jnp.float32)
        * inverse_in
        * gain_piece
    ).astype(jnp.bfloat16)
    pre_u = jnp.dot(normed_piece, full_u, preferred_element_type=jnp.float32)
    pre_v = jnp.dot(normed_piece, full_v, preferred_element_type=jnp.float32)
    gate_u = jax.nn.gelu(pre_u * scale_u)
    act_v = jax.nn.gelu(pre_v * scale_v)
    local_width = act_v.shape[1]
    row_sums, row_squares = lax.psum((jnp.sum(act_v, axis=1), jnp.sum(act_v * act_v, axis=1)), "tp")
    row_mean = (row_sums / GM_W)[:, None]
    square = (row_squares / GM_W)[:, None]
    v_norm = (
        (act_v - row_mean) * lax.rsqrt(square - row_mean * row_mean + 1e-06) * mix_gain
    ).astype(jnp.bfloat16)
    group_index = lax.axis_index("tp") * local_width // (GM_W // GROUPS)
    lower_mask = jnp.tril(jnp.ones((BLOCK, BLOCK), jnp.float32))
    spatial_mask = (
        lax.dynamic_index_in_dim(spatial_weight, group_index, 0, keepdims=False) * lower_mask
    ).astype(jnp.bfloat16)
    block_bias = lax.dynamic_index_in_dim(spatial_bias, group_index, 0, keepdims=False)
    blocks = v_norm.reshape(-1, BLOCK, local_width)
    mixed_cols = jnp.einsum("ts,nsc->ntc", spatial_mask, blocks, preferred_element_type=jnp.float32)
    mixed_cols = mixed_cols + block_bias[None, :, None]
    gated = (gate_u * mixed_cols.reshape(-1, local_width)).astype(jnp.bfloat16)
    out_rounded = weight_out.astype(jnp.bfloat16)
    full_out = lax.all_gather(out_rounded, "fs", axis=1, tiled=True)
    columns = full_out
    piece_scale = out_scales
    product = lax.dot_general(
        columns, gated, (((0,), (1,)), ((), ())), preferred_element_type=jnp.float32
    )
    mixer_sum = (
        lax.psum_scatter(
            (product * piece_scale[:, None]).astype(jnp.bfloat16),
            "tp",
            scatter_dimension=0,
            tiled=True,
        )
        .astype(jnp.float32)
        .T
    )
    residual = (tokens.astype(jnp.float32) + mixer_sum).astype(jnp.bfloat16)
    full_up = lax.all_gather(weight_up.astype(jnp.bfloat16), "fs", axis=0, tiled=True)
    widened_mid = residual.astype(jnp.float32)
    squares_mid = lax.psum(jnp.sum(widened_mid * widened_mid, axis=1), "tp")
    inverse_mid = lax.rsqrt(squares_mid / feature_count + 1e-06)[:, None]
    gain_piece = norm2_gain
    normed_piece = (
        lax.all_gather(residual, "tp", axis=1, tiled=True).astype(jnp.float32)
        * inverse_mid
        * gain_piece
    ).astype(jnp.bfloat16)
    pre_up = jnp.dot(normed_piece, full_up, preferred_element_type=jnp.float32)
    hidden = jnp.square(jax.nn.relu(pre_up * scale_up)).astype(jnp.bfloat16)
    down_rounded = weight_down.astype(jnp.bfloat16)
    full_down = lax.all_gather(down_rounded, "fs", axis=1, tiled=True)
    columns = full_down
    piece_scale = down_scales
    product = lax.dot_general(
        columns, hidden, (((0,), (1,)), ((), ())), preferred_element_type=jnp.float32
    )
    channel_sum = (
        lax.psum_scatter(
            (product * piece_scale[:, None]).astype(jnp.bfloat16),
            "tp",
            scatter_dimension=0,
            tiled=True,
        )
        .astype(jnp.float32)
        .T
    )
    return (residual.astype(jnp.float32) + channel_sum).astype(jnp.bfloat16)


def solution(mesh):
    placed = (
        P(("grp", "fs"), "tp"),
        P(),
        P("fs", "tp"),
        P("fs", "tp"),
        P("tp"),
        P("tp"),
        P("tp"),
        P(),
        P(),
        P("tp", "fs"),
        P("fs"),
        P(),
        P("fs", "tp"),
        P("tp"),
        P("tp", "fs"),
        P("fs"),
    )
    return jax.shard_map(
        per_device, mesh=mesh, in_specs=placed, out_specs=P(("grp", "fs"), "tp"), check_vma=False
    )
```

profile of v0, /device:TPU:0, one launch (start us, length us, event | category | flops | bytes accessed | tf_op | source)
XLA Modules:
  0.0 601.0 jit_solution(15916655100287442903)
XLA Ops:
  6.5 1.8 convert_element_type.74
  9.1 1.8 convert_element_type.73
  11.0 1.8 convert_element_type.79
  14.3 8.4 %psum.28 = f32[1024]{0:T(1024)S(1)} all-reduce(f32[1024]{0:T(1024)S(1)} %fusion.8), channel_id=1, replica_groups=mesh['grp'=2,'fs'=4,'tp'=4] {'tp'}, use_global_device_ids=true, to_apply=%region_1.0 | all-reduce | flops 1024 | bytes 8192 | tf_op jit(solution)/shard_map/psum | solution.py:39
  22.7 12.7 %all-gather = f32[4,1,512]{2,1,0:T(1,128)S(1)} all-gather(f32[1,1,512]{2,1,0:T(1,128)} %bitcast.33), channel_id=1, replica_groups=mesh['grp'=2,'fs'=4,'tp'=4] {'fs'}, dimensions={0}, use_global_device_ids=true | all-gather | bytes 10240 | tf_op jit(solution)/shard_map/all_gather | solution.py:31
  35.5 4.3 all-gather.14.cloned.1.call-done
  39.8 35.4 %all-gather.10.cloned.1.call-done = bf16[1024,2048]{1,0:T(8,128)(2,1)} async-done(((bf16[1024,512]{1,0:T(8,128)(2,1)}), bf16[1024,2048]{1,0:T(8,128)(2,1)}) %all-gather.10.cloned.1.call-update) | async-done | bytes 4194320 | tf_op jit(solution)/shard_map/all_gather | solution.py:43
  75.2 4.2 fusion.45
  79.4 6.0 %all-reduce = (f32[1024]{0:T(1024)S(1)}, f32[1024]{0:T(1024)S(1)}) all-reduce(f32[1024]{0:T(1024)S(1)} %get-tuple-element.6, f32[1024]{0:T(1024)S(1)} %get-tuple-element.5), channel_id=1, replica_groups=mesh['grp'=2,'fs'=4,'tp'=4] {'tp'}, use_global_device_ids=true, to_apply=%region_5.0 | all-reduce | flops 2048 | bytes 16384 | tf_op jit(solution)/shard_map/psum | solution.py:52
  86.9 17.9 %all-gather.12.cloned.1.call-done = bf16[2048,256]{1,0:T(8,128)(2,1)} async-done(((bf16[512,256]{1,0:T(8,128)(2,1)}), bf16[2048,256]{1,0:T(8,128)(2,1)}) %all-gather.12.cloned.1.call-update) | async-done | bytes 1048592 | tf_op jit(solution)/shard_map/all_gather | solution.py:35
  104.8 28.8 %all-gather.16.cloned.1.call-done = bf16[256,2048]{1,0:T(8,128)(2,1)} async-done(((bf16[256,512]{1,0:T(8,128)(2,1)}), bf16[256,2048]{1,0:T(8,128)(2,1)}) %all-gather.16.cloned.1.call-update) | async-done | bytes 1048592 | tf_op jit(solution)/shard_map/all_gather | solution.py:69
  133.6 9.3 %fusion.6 = bf16[2048,1024]{0,1:T(8,128)(2,1)} fusion(f32[2048]{0:T(1024)S(1)} %bitcast.31, bf16[256,2048]{1,0:T(8,128)(2,1)} %all-gather.16.cloned.1.call-done, f32[1024,256]{1,0:T(8,128)S(1)} %bitcast.30, bf16[2048,256]{1,0:T(8,128)(2,1)} %all-gather.12.cloned.1.call-done, bf16[1024,2048]{1,0:T(8,128)(2,1)} %all-gather.10.cloned.1.call-done, ...), kind=kOutput, calls=%fused_computation.9 | convolution fusion | flops 2162950144 | bytes 11555840 | tf_op jit(solution)/shard_map/dot_general | solution.py:72
  143.0 3.9 convert_element_type.86
  147.0 4.4 convert_element_type.88
  151.5 35.4 %reduce-scatter.3.cloned.1.call-done = bf16[512,1024]{0,1:T(8,128)(2,1)} async-done(((bf16[2048,1024]{0,1:T(8,128)(2,1)}), bf16[512,1024]{0,1:T(8,128)(2,1)}) %reduce-scatter.3.cloned.1.call-update) | async-done | bytes 1048592 | tf_op jit(solution)/shard_map/reduce_scatter | solution.py:76
  186.8 2.6 fusion.10
  189.5 12.0 %all-gather.1 = f32[4,1,512]{2,1,0:T(1,128)S(1)} all-gather(f32[1,1,512]{2,1,0:T(1,128)S(1)} %bitcast.34), channel_id=1, replica_groups=mesh['grp'=2,'fs'=4,'tp'=4] {'fs'}, dimensions={0}, use_global_device_ids=true | all-gather | bytes 10240 | tf_op jit(solution)/shard_map/all_gather | solution.py:32
  201.5 6.0 %psum.31 = f32[1024]{0:T(1024)S(1)} all-reduce(f32[1024]{0:T(1024)S(1)} %get-tuple-element.9), channel_id=1, replica_groups=mesh['grp'=2,'fs'=4,'tp'=4] {'tp'}, use_global_device_ids=true, to_apply=%region_8.9 | all-reduce | flops 1024 | bytes 8192 | tf_op jit(solution)/shard_map/psum | solution.py:88
  207.6 130.4 %all-gather.20.cloned.1.call-done = bf16[2048,2048]{1,0:T(8,128)(2,1)} async-done(((bf16[512,2048]{1,0:T(8,128)(2,1)}), bf16[2048,2048]{1,0:T(8,128)(2,1)}) %all-gather.20.cloned.1.call-update) | async-done | bytes 8388624 | tf_op jit(solution)/shard_map/all_gather | solution.py:86
  337.9 149.4 %all-gather.22.cloned.1.call-done = bf16[2048,2048]{1,0:T(8,128)(2,1)} async-done(((bf16[2048,512]{1,0:T(8,128)(2,1)}), bf16[2048,2048]{1,0:T(8,128)(2,1)}) %all-gather.22.cloned.1.call-update) | async-done | bytes 8388624 | tf_op jit(solution)/shard_map/all_gather | solution.py:99
  487.3 34.2 %all-gather.18.cloned.1.call-done = bf16[1024,2048]{1,0:T(8,128)(2,1)} async-done(((bf16[1024,512]{1,0:T(8,128)(2,1)}), bf16[1024,2048]{1,0:T(8,128)(2,1)}) %all-gather.18.cloned.1.call-update) | async-done | bytes 4194320 | tf_op jit(solution)/shard_map/all_gather | solution.py:92
  521.6 25.7 %fusion.7 = bf16[2048,1024]{0,1:T(8,128)(2,1)} fusion(f32[2048]{0:T(1024)S(1)} %bitcast.32, bf16[2048,2048]{1,0:T(8,128)(2,1)} %all-gather.22.cloned.1.call-done, bf16[2048,2048]{1,0:T(8,128)(2,1)} %all-gather.20.cloned.1.call-done, bf16[1024,2048]{1,0:T(8,128)(2,1)} %all-gather.18.cloned.1.call-done, f32[2048]{0:T(1024)S(1)} %copy-done.6, ...), kind=kOutput, calls=%fused_computation.10 | convolution fusion | flops 17200840704 | bytes 25194496 | tf_op jit(solution)/shard_map/dot_general | solution.py:102
  547.3 44.6 %reduce-scatter.5.cloned.1.call-done = bf16[512,1024]{0,1:T(8,128)(2,1)} async-done(((bf16[2048,1024]{0,1:T(8,128)(2,1)}), bf16[512,1024]{0,1:T(8,128)(2,1)}) %reduce-scatter.5.cloned.1.call-update) | async-done | bytes 1048592 | tf_op jit(solution)/shard_map/reduce_scatter | solution.py:106
  591.9 2.5 fusion.11
  (43 shorter events, 4.2 us)
Async XLA Ops:
  6.5 28.9 %copy-start = (f32[4,128]{1,0:T(4,128)S(1)}, f32[4,128]{1,0:T(4,128)}, u32[]{:S(2)}) copy-start(f32[4,128]{1,0:T(4,128)} %param.24) | copy-start | bytes 6148
  6.5 33.2 %all-gather.14.cloned.1.call-start = ((), (), s32[]{:S(2)}) async-start(), calls=%async_computation.4 | async-start | bytes 1310720 | tf_op jit(solution)/shard_map/all_gather | solution.py:36
  8.3 66.9 %all-gather.10.cloned.1.call-start = ((), (), s32[]{:S(2)}) async-start(), calls=%async_computation.2 | async-start | bytes 5242880 | tf_op jit(solution)/shard_map/all_gather | solution.py:43
  9.1 95.7 %all-gather.12.cloned.1.call-start = ((), (), s32[]{:S(2)}) async-start(), calls=%async_computation.3 | async-start | bytes 1310720 | tf_op jit(solution)/shard_map/all_gather | solution.py:35
  10.9 122.7 %all-gather.16.cloned.1.call-start = ((), (), s32[]{:S(2)}) async-start(), calls=%async_computation.5 | async-start | bytes 1310720 | tf_op jit(solution)/shard_map/all_gather | solution.py:69
  12.8 174.1 %reduce-scatter.3.cloned.1.call-start = ((), (), s32[]{:S(2)}) async-start(), calls=%async_computation.6 | async-start | bytes 5242880 | tf_op jit(solution)/shard_map/reduce_scatter | solution.py:76
  35.4 50.0 %copy-start.4 = (f32[256]{0:T(256)S(1)}, f32[256]{0:T(256)}, u32[]{:S(2)}) copy-start(f32[256]{0:T(256)} %param.22) | copy-start | bytes 3076
  35.4 98.2 %copy-start.5 = (f32[2048]{0:T(1024)S(1)}, f32[2048]{0:T(1024)}, u32[]{:S(2)}) copy-start(f32[2048]{0:T(1024)} %param.17) | copy-start | bytes 24580
  35.4 98.2 %copy-start.8 = (f32[256]{0:T(256)S(1)}, f32[256]{0:T(256)}, u32[]{:S(2)}) copy-start(f32[256]{0:T(256)} %param.20) | copy-start | bytes 3076
  142.9 43.9 %copy-start.2 = (bf16[1024,512]{1,0:T(8,128)(2,1)S(1)}, bf16[1024,512]{1,0:T(8,128)(2,1)}, u32[]{:S(2)}) copy-start(bf16[1024,512]{1,0:T(8,128)(2,1)} %param.16) | copy-start | bytes 3145732
  142.9 195.0 %all-gather.20.cloned.1.call-start = ((), (), s32[]{:S(2)}) async-start(), calls=%async_computation.8 | async-start | bytes 10485760 | tf_op jit(solution)/shard_map/all_gather | solution.py:86
  146.9 42.6 %copy-start.3 = (f32[512]{0:T(512)S(1)}, f32[512]{0:T(512)}, u32[]{:S(2)}) copy-start(f32[512]{0:T(512)} %param.31) | copy-start | bytes 6148
  146.9 374.6 %copy-start.6 = (f32[2048]{0:T(1024)S(1)}, f32[2048]{0:T(1024)}, u32[]{:S(2)}) copy-start(f32[2048]{0:T(1024)} %param.29) | copy-start | bytes 24580
  146.9 374.6 %copy-start.7 = (f32[2048]{0:T(1024)S(1)}, f32[2048]{0:T(1024)}, u32[]{:S(2)}) copy-start(f32[2048]{0:T(1024)} %param.27) | copy-start | bytes 24580
  146.9 340.4 %all-gather.22.cloned.1.call-start = ((), (), s32[]{:S(2)}) async-start(), calls=%async_computation.9 | async-start | bytes 10485760 | tf_op jit(solution)/shard_map/all_gather | solution.py:99
  151.4 370.1 %all-gather.18.cloned.1.call-start = ((), (), s32[]{:S(2)}) async-start(), calls=%async_computation.7 | async-start | bytes 5242880 | tf_op jit(solution)/shard_map/all_gather | solution.py:92
  189.5 402.4 %reduce-scatter.5.cloned.1.call-start = ((), (), s32[]{:S(2)}) async-start(), calls=%async_computation.10 | async-start | bytes 5242880 | tf_op jit(solution)/shard_map/reduce_scatter | solution.py:106
  521.6 70.3 %copy-start.1 = (bf16[1024,512]{1,0:T(8,128)(2,1)S(1)}, bf16[1024,512]{1,0:T(8,128)(2,1)}, u32[]{:S(2)}) copy-start(bf16[1024,512]{1,0:T(8,128)(2,1)} %get-tuple-element.10) | copy-start | bytes 3145732
Sparse Core Ops, SparseCore 0:
  8.9 30.8 all-gather.13
  41.3 33.8 all-gather.9
  76.8 27.9 all-gather.11
  106.2 27.3 all-gather.15
  143.1 43.7 reduce-scatter.2
  188.3 149.6 all-gather.19
  339.5 147.7 all-gather.21
  488.9 32.6 all-gather.17
  547.5 44.3 reduce-scatter.4
where the time goes:
time: 601 us
  waiting for transfers between devices  481 us (80%)
  blocking collectives  45.1 us (8%)
  matrix products  40.3 us (7%)
  other arithmetic  20.6 us (3%)
  between operations  13.3 us (2%)
    all_gather x1, waiting for transfers between devices, per_device(): full_down = lax.all_gather(down_rounded, 'fs', axis=1, tiled=True)  149 us
    all_gather x1, waiting for transfers between devices, per_device(): lax.all_gather(weight_up.astype(jnp.bfloat16), 'fs', axis=0, tiled=True)  130 us
    reduce_scatter x2, waiting for transfers between devices, per_device(): lax.psum_scatter((product * piece_scale[:, None]).astype(jnp.bfloat16), '...  79.9 us
    all_gather x1, waiting for transfers between devices, per_device(): lax.all_gather(tokens, 'tp', axis=1, tiled=True).astype(jnp.float32)  35.4 us
    all_gather x1, waiting for transfers between devices, per_device(): lax.all_gather(residual, 'tp', axis=1, tiled=True).astype(jnp.float32)  34.2 us
    all_gather x1, waiting for transfers between devices, per_device(): full_out = lax.all_gather(out_rounded, 'fs', axis=1, tiled=True)  28.8 us
    dot_general x1, matrix products, per_device(): lax.dot_general(columns, hidden, (((0,), (1,)), ((), ())), preferred_elem...  25.7 us
    all_gather x1, waiting for transfers between devices, per_device(): lax.all_gather(weight_u.astype(jnp.bfloat16), 'fs', axis=0, tiled=True)  17.9 us
  transfers between devices with their start and end apart: 9, of which 9 were waited for; matrix products, arithmetic and copies ran while one was open for 4% of the time, Pallas kernels for 0%

commit v1 on v0

--- a/solution.py
+++ b/solution.py
@@ -6,6 +6,19 @@
 GM_W = 1024
 GROUPS = 4
 BLOCK = 128
+
+
+def gather_around(x, axis, dim):
+    ways = lax.axis_size(axis)
+    up = [(d, (d + 1) % ways) for d in range(ways)]
+    down = [(d, (d - 1) % ways) for d in range(ways)]
+    earlier, later = ([x], [x])
+    for _ in range(ways // 2):
+        earlier.append(lax.ppermute(earlier[-1], axis, up))
+    for _ in range((ways - 1) // 2):
+        later.append(lax.ppermute(later[-1], axis, down))
+    line = jnp.concatenate([*earlier[::-1], *later[1:]], axis=dim)
+    return jnp.roll(line, (lax.axis_index(axis) - ways // 2) * x.shape[dim], axis=dim)
 
 
 def per_device(
@@ -89,9 +102,7 @@
     inverse_mid = lax.rsqrt(squares_mid / feature_count + 1e-06)[:, None]
     gain_piece = norm2_gain
     normed_piece = (
-        lax.all_gather(residual, "tp", axis=1, tiled=True).astype(jnp.float32)
-        * inverse_mid
-        * gain_piece
+        gather_around(residual, "tp", 1).astype(jnp.float32) * inverse_mid * gain_piece
     ).astype(jnp.bfloat16)
     pre_up = jnp.dot(normed_piece, full_up, preferred_element_type=jnp.float32)
     hidden = jnp.square(jax.nn.relu(pre_up * scale_up)).astype(jnp.bfloat16)

time: 601 us -> 566 us (0.942)
  waiting for transfers between devices: 481 us -> 426 us
  local copies, waits for them, and re-layouts: 0.05 us -> 11.5 us
  blocking collectives: 45.1 us -> 52.3 us
    all_gather x1 -> x0, waiting for transfers between devices: 34.2 us -> none  [per_device(): lax.all_gather(residual, 'tp', axis=1, tiled=True).astype(jnp.float32)]
    all_gather x1, waiting for transfers between devices: 130 us -> 96.7 us  [per_device(): lax.all_gather(weight_up.astype(jnp.bfloat16), 'fs', axis=0, tiled=True)]
    ppermute x0 -> x3, waiting for transfers between devices: none -> 14.2 us  [the longest x2 14.2 us: gather_around(): earlier.append(lax.ppermute(earlier[-1], axis, up))]
    unnamed x18 -> x25, local copies, waits for them, and re-layouts: 0.04 us -> 10.4 us
  transfers between devices with their start and end apart: 9 -> 11, of which waited for: 9 -> 9; matrix products, arithmetic and copies ran while one was open for 4% -> 6% of each run, Pallas kernels for 0% -> 0%
where the time goes in v1:
time: 566 us; the launch traced here: 565 us
  waiting for transfers between devices  426 us (75%)
  blocking collectives  52.3 us (9%)
  matrix products  40.3 us (7%)
  other arithmetic  19.7 us (3%)
  between operations  13.7 us (2%)
  local copies, waits for them, and re-layouts  11.5 us (2%)
    all_gather x1, waiting for transfers between devices, per_device(): full_down = lax.all_gather(down_rounded, 'fs', axis=1, tiled=True)  149 us
    all_gather x1, waiting for transfers between devices, per_device(): lax.all_gather(weight_up.astype(jnp.bfloat16), 'fs', axis=0, tiled=True)  96.7 us
    reduce_scatter x2, waiting for transfers between devices, per_device(): lax.psum_scatter((product * piece_scale[:, None]).astype(jnp.bfloat16), '...  78.1 us
    all_gather x1, waiting for transfers between devices, per_device(): lax.all_gather(tokens, 'tp', axis=1, tiled=True).astype(jnp.float32)  35.4 us
    all_gather x1, waiting for transfers between devices, per_device(): full_out = lax.all_gather(out_rounded, 'fs', axis=1, tiled=True)  28.8 us
    dot_general x1, matrix products, per_device(): lax.dot_general(columns, hidden, (((0,), (1,)), ((), ())), preferred_elem...  25.7 us
    all_gather x1, waiting for transfers between devices, per_device(): lax.all_gather(weight_u.astype(jnp.bfloat16), 'fs', axis=0, tiled=True)  17.9 us
    ppermute x2, waiting for transfers between devices, gather_around(): earlier.append(lax.ppermute(earlier[-1], axis, up))  14.2 us
  transfers between devices with their start and end apart: 11, of which 9 were waited for; matrix products, arithmetic and copies ran while one was open for 6% of the time, Pallas kernels for 0%

profile of v1, /device:TPU:0, one launch (start us, length us, event | category | flops | bytes accessed | tf_op | source)
XLA Modules:
  0.0 565.3 jit_solution(6685994092567540132)
XLA Ops:
  6.5 1.8 convert_element_type.74
  11.0 1.8 convert_element_type.79
  14.4 8.4 %psum.28 = f32[1024]{0:T(1024)S(1)} all-reduce(f32[1024]{0:T(1024)S(1)} %fusion.10), channel_id=1, replica_groups=mesh['grp'=2,'fs'=4,'tp'=4] {'tp'}, use_global_device_ids=true, to_apply=%region_1.0 | all-reduce | flops 1024 | bytes 8192 | tf_op jit(solution)/shard_map/psum | solution.py:52
  22.7 12.7 %all-gather = f32[4,1,512]{2,1,0:T(1,128)S(1)} all-gather(f32[1,1,512]{2,1,0:T(1,128)} %bitcast.33), channel_id=1, replica_groups=mesh['grp'=2,'fs'=4,'tp'=4] {'fs'}, dimensions={0}, use_global_device_ids=true | all-gather | bytes 10240 | tf_op jit(solution)/shard_map/all_gather | solution.py:44
  35.5 4.3 all-gather.13.cloned.1.call-done
  39.8 35.4 %all-gather.9.cloned.1.call-done = bf16[1024,2048]{1,0:T(8,128)(2,1)} async-done(((bf16[1024,512]{1,0:T(8,128)(2,1)}), bf16[1024,2048]{1,0:T(8,128)(2,1)}) %all-gather.9.cloned.1.call-update) | async-done | bytes 4194320 | tf_op jit(solution)/shard_map/all_gather | solution.py:56
  75.2 4.2 fusion.50
  79.4 6.0 %all-reduce = (f32[1024]{0:T(1024)S(1)}, f32[1024]{0:T(1024)S(1)}) all-reduce(f32[1024]{0:T(1024)S(1)} %get-tuple-element.6, f32[1024]{0:T(1024)S(1)} %get-tuple-element.5), channel_id=1, replica_groups=mesh['grp'=2,'fs'=4,'tp'=4] {'tp'}, use_global_device_ids=true, to_apply=%region_5.0 | all-reduce | flops 2048 | bytes 16384 | tf_op jit(solution)/shard_map/psum | solution.py:65
  86.9 17.9 %all-gather.11.cloned.1.call-done = bf16[2048,256]{1,0:T(8,128)(2,1)} async-done(((bf16[512,256]{1,0:T(8,128)(2,1)}), bf16[2048,256]{1,0:T(8,128)(2,1)}) %all-gather.11.cloned.1.call-update) | async-done | bytes 1048592 | tf_op jit(solution)/shard_map/all_gather | solution.py:48
  104.8 28.8 %all-gather.15.cloned.1.call-done = bf16[256,2048]{1,0:T(8,128)(2,1)} async-done(((bf16[256,512]{1,0:T(8,128)(2,1)}), bf16[256,2048]{1,0:T(8,128)(2,1)}) %all-gather.15.cloned.1.call-update) | async-done | bytes 1048592 | tf_op jit(solution)/shard_map/all_gather | solution.py:82
  133.6 9.3 %fusion.8 = bf16[2048,1024]{0,1:T(8,128)(2,1)} fusion(f32[2048]{0:T(1024)S(1)} %bitcast.31, bf16[256,2048]{1,0:T(8,128)(2,1)} %all-gather.15.cloned.1.call-done, f32[1024,256]{1,0:T(8,128)S(1)} %bitcast.30, bf16[2048,256]{1,0:T(8,128)(2,1)} %all-gather.11.cloned.1.call-done, bf16[1024,2048]{1,0:T(8,128)(2,1)} %all-gather.9.cloned.1.call-done, ...), kind=kOutput, calls=%fused_computation.10 | convolution fusion | flops 2162950144 | bytes 11555840 | tf_op jit(solution)/shard_map/dot_general | solution.py:85
  143.0 3.9 convert_element_type.86
  147.0 4.4 convert_element_type.88
  151.5 35.4 %reduce-scatter.3.cloned.1.call-done = bf16[512,1024]{0,1:T(8,128)(2,1)} async-done(((bf16[2048,1024]{0,1:T(8,128)(2,1)}), bf16[512,1024]{0,1:T(8,128)(2,1)}) %reduce-scatter.3.cloned.1.call-update) | async-done | bytes 1048592 | tf_op jit(solution)/shard_map/reduce_scatter | solution.py:89
  188.6 14.2 %collective-permute-done = bf16[1024,512]{1,0:T(8,128)(2,1)S(1)} collective-permute-done((bf16[1024,512]{1,0:T(8,128)(2,1)S(1)}, bf16[1024,512]{1,0:T(8,128)(2,1)S(1)}, u32[]{:S(2)}, u32[]{:S(2)}) %collective-permute-start) | collective-permute-done | bytes 1048608 | tf_op jit(solution)/shard_map/ppermute | solution.py:17
  204.6 14.1 %all-gather.1 = f32[4,1,512]{2,1,0:T(1,128)S(1)} all-gather(f32[1,1,512]{2,1,0:T(1,128)S(1)} %bitcast.34), channel_id=1, replica_groups=mesh['grp'=2,'fs'=4,'tp'=4] {'fs'}, dimensions={0}, use_global_device_ids=true | all-gather | bytes 10240 | tf_op jit(solution)/shard_map/all_gather | solution.py:45
  218.7 11.2 %psum.31 = f32[1024]{0:T(1024)S(1)} all-reduce(f32[1024]{0:T(1024)S(1)} %get-tuple-element.9), channel_id=1, replica_groups=mesh['grp'=2,'fs'=4,'tp'=4] {'tp'}, use_global_device_ids=true, to_apply=%region_8.9 | all-reduce | flops 1024 | bytes 8192 | tf_op jit(solution)/shard_map/psum | solution.py:101
  229.9 2.3 constant_dynamic-update-slice_fusion.7
  235.6 2.3 constant_dynamic-update-slice_fusion.3
  241.3 96.7 %all-gather.17.cloned.1.call-done = bf16[2048,2048]{1,0:T(8,128)(2,1)} async-done(((bf16[512,2048]{1,0:T(8,128)(2,1)}), bf16[2048,2048]{1,0:T(8,128)(2,1)}) %all-gather.17.cloned.1.call-update) | async-done | bytes 8388624 | tf_op jit(solution)/shard_map/all_gather | solution.py:99
  338.1 149.4 %all-gather.19.cloned.1.call-done = bf16[2048,2048]{1,0:T(8,128)(2,1)} async-done(((bf16[2048,512]{1,0:T(8,128)(2,1)}), bf16[2048,2048]{1,0:T(8,128)(2,1)}) %all-gather.19.cloned.1.call-update) | async-done | bytes 8388624 | tf_op jit(solution)/shard_map/all_gather | solution.py:110
  487.5 25.7 %fusion.9 = bf16[2048,1024]{0,1:T(8,128)(2,1)} fusion(f32[2048]{0:T(1024)S(1)} %bitcast.32, bf16[2048,2048]{1,0:T(8,128)(2,1)} %all-gather.19.cloned.1.call-done, bf16[2048,2048]{1,0:T(8,128)(2,1)} %all-gather.17.cloned.1.call-done, f32[2048]{0:T(1024)S(1)} %copy-done.6, f32[2048]{0:T(1024)S(1)} %copy-done.7, f32[1024]{0:T(1024)S(1)} %add_rsqrt_fusion, ...), kind=kOutput, calls=%fused_computation.11 | convolution fusion | flops 17200840704 | bytes 25194500 | tf_op jit(solution)/shard_map/dot_general | solution.py:113
  513.1 42.7 %reduce-scatter.5.cloned.1.call-done = bf16[512,1024]{0,1:T(8,128)(2,1)} async-done(((bf16[2048,1024]{0,1:T(8,128)(2,1)}), bf16[512,1024]{0,1:T(8,128)(2,1)}) %reduce-scatter.5.cloned.1.call-update) | async-done | bytes 1048592 | tf_op jit(solution)/shard_map/reduce_scatter | solution.py:117
  555.9 2.5 fusion.13
  (54 shorter events, 16.2 us)
Async XLA Ops:
  6.5 28.9 %copy-start = (f32[4,128]{1,0:T(4,128)S(1)}, f32[4,128]{1,0:T(4,128)}, u32[]{:S(2)}) copy-start(f32[4,128]{1,0:T(4,128)} %param.24) | copy-start | bytes 6148
  6.5 33.2 %all-gather.13.cloned.1.call-start = ((), (), s32[]{:S(2)}) async-start(), calls=%async_computation.4 | async-start | bytes 1310720 | tf_op jit(solution)/shard_map/all_gather | solution.py:49
  8.3 66.9 %all-gather.9.cloned.1.call-start = ((), (), s32[]{:S(2)}) async-start(), calls=%async_computation.2 | async-start | bytes 5242880 | tf_op jit(solution)/shard_map/all_gather | solution.py:56
  9.1 95.7 %all-gather.11.cloned.1.call-start = ((), (), s32[]{:S(2)}) async-start(), calls=%async_computation.3 | async-start | bytes 1310720 | tf_op jit(solution)/shard_map/all_gather | solution.py:48
  10.9 122.7 %all-gather.15.cloned.1.call-start = ((), (), s32[]{:S(2)}) async-start(), calls=%async_computation.5 | async-start | bytes 1310720 | tf_op jit(solution)/shard_map/all_gather | solution.py:82
  12.8 174.1 %reduce-scatter.3.cloned.1.call-start = ((), (), s32[]{:S(2)}) async-start(), calls=%async_computation.6 | async-start | bytes 5242880 | tf_op jit(solution)/shard_map/reduce_scatter | solution.py:89
  35.4 50.0 %copy-start.4 = (f32[256]{0:T(256)S(1)}, f32[256]{0:T(256)}, u32[]{:S(2)}) copy-start(f32[256]{0:T(256)} %param.22) | copy-start | bytes 3076
  35.4 98.2 %copy-start.5 = (f32[2048]{0:T(1024)S(1)}, f32[2048]{0:T(1024)}, u32[]{:S(2)}) copy-start(f32[2048]{0:T(1024)} %param.17) | copy-start | bytes 24580
  35.4 98.2 %copy-start.8 = (f32[256]{0:T(256)S(1)}, f32[256]{0:T(256)}, u32[]{:S(2)}) copy-start(f32[256]{0:T(256)} %param.20) | copy-start | bytes 3076
  142.9 43.9 %copy-start.2 = (bf16[1024,512]{1,0:T(8,128)(2,1)S(1)}, bf16[1024,512]{1,0:T(8,128)(2,1)}, u32[]{:S(2)}) copy-start(bf16[1024,512]{1,0:T(8,128)(2,1)} %param.16) | copy-start | bytes 3145732
  142.9 195.1 %all-gather.17.cloned.1.call-start = ((), (), s32[]{:S(2)}) async-start(), calls=%async_computation.7 | async-start | bytes 10485760 | tf_op jit(solution)/shard_map/all_gather | solution.py:99
  146.9 57.6 %copy-start.3 = (f32[512]{0:T(512)S(1)}, f32[512]{0:T(512)}, u32[]{:S(2)}) copy-start(f32[512]{0:T(512)} %param.31) | copy-start | bytes 6148
  147.0 340.5 %all-gather.19.cloned.1.call-start = ((), (), s32[]{:S(2)}) async-start(), calls=%async_computation.8 | async-start | bytes 10485760 | tf_op jit(solution)/shard_map/all_gather | solution.py:110
  151.4 404.5 %reduce-scatter.5.cloned.1.call-start = ((), (), s32[]{:S(2)}) async-start(), calls=%async_computation.9 | async-start | bytes 5242880 | tf_op jit(solution)/shard_map/reduce_scatter | solution.py:117
  188.6 14.3 %collective-permute-start = (bf16[1024,512]{1,0:T(8,128)(2,1)S(1)}, bf16[1024,512]{1,0:T(8,128)(2,1)S(1)}, u32[]{:S(2)}, u32[]{:S(2)}) collective-permute-start(bf16[1024,512]{1,0:T(8,128)(2,1)S(1)} %get-tuple-element.10), channel_id=1, source_target_pairs={{0,1},{1,2},{2,3},{3,0},{4,5},{5,6},{6,7},{7,4},{8,9},{9,10},{10,1... | collective-permute-start | bytes 3145736 | tf_op jit(solution)/shard_map/ppermute | solution.py:17
  202.8 27.1 %collective-permute-start.1 = (bf16[1024,512]{1,0:T(8,128)(2,1)S(1)}, bf16[1024,512]{1,0:T(8,128)(2,1)}, u32[]{:S(2)}, u32[]{:S(2)}) collective-permute-start(bf16[1024,512]{1,0:T(8,128)(2,1)S(1)} %collective-permute-done), channel_id=1, source_target_pairs={{0,1},{1,2},{2,3},{3,0},{4,5},{5,6},{6,7},{7,4},{8,9},{9,10},{10,1... | collective-permute-start | bytes 3145736 | tf_op jit(solution)/shard_map/ppermute | solution.py:17
  202.8 31.6 %collective-permute-start.2 = (bf16[1024,512]{1,0:T(8,128)(2,1)S(1)}, bf16[1024,512]{1,0:T(8,128)(2,1)S(1)}, u32[]{:S(2)}, u32[]{:S(2)}) collective-permute-start(bf16[1024,512]{1,0:T(8,128)(2,1)S(1)} %get-tuple-element.10), channel_id=1, source_target_pairs={{0,3},{1,0},{2,1},{3,2},{4,7},{5,4},{6,5},{7,6},{8,11},{9,8},{10,9... | collective-permute-start | bytes 3145736 | tf_op jit(solution)/shard_map/ppermute | solution.py:19
  229.9 257.6 %copy-start.6 = (f32[2048]{0:T(1024)S(1)}, f32[2048]{0:T(1024)}, u32[]{:S(2)}) copy-start(f32[2048]{0:T(1024)} %param.29) | copy-start | bytes 24580
  229.9 257.6 %copy-start.7 = (f32[2048]{0:T(1024)S(1)}, f32[2048]{0:T(1024)}, u32[]{:S(2)}) copy-start(f32[2048]{0:T(1024)} %param.27) | copy-start | bytes 24580
  487.5 71.0 %copy-start.1 = (f32[4,128]{1,0:T(4,128)S(1)}, f32[4,128]{1,0:T(4,128)}, u32[]{:S(2)}) copy-start(f32[4,128]{1,0:T(4,128)} %param.24) | copy-start | bytes 6148
Sparse Core Ops, SparseCore 0:
  8.9 30.8 all-gather.12
  41.3 33.8 all-gather.8
  76.8 27.9 all-gather.10
  106.2 27.3 all-gather.14
  143.1 43.7 reduce-scatter.2
  188.3 149.7 all-gather.16
  339.6 147.7 all-gather.18
  513.3 42.5 reduce-scatter.4
